TPU v7x, 512 devices: a whole 4x4x16 slice. The times are simulated.
512 devices in a mesh: fs: 16 (over z), rep: 4 (over y), tp: 8 (over x, core).
Axes of the slice: x: 4, y: 4, z: 16, core: 2. Of those that a mesh axis runs over, the one named last changes fastest.
Arguments:
- normed_input: bfloat16 [8192, 1024], P(('fs', 'rep')), may hold values from -6 to 6
- query_cotangent: bfloat16 [8192, 512], P(('fs', 'rep'), 'tp'), may hold values from -0.029907227 to 0.029907227
- value_cotangent: bfloat16 [8192, 1024], P(('fs', 'rep'), 'tp'), may hold values from -0.029907227 to 0.029907227
- query_basis: bfloat16 [1024, 128], replicated, may hold values from -0.1875 to 0.1875
- value_basis: bfloat16 [1024, 128], replicated, may hold values from -0.1875 to 0.1875
- query_weight: float32 [1024, 512], P(('fs', 'rep'), 'tp'), may hold values from -0.1875 to 0.1875
- value_weight: float32 [1024, 1024], P(('fs', 'rep'), 'tp'), may hold values from -0.1875 to 0.1875
- query_first: float32 [128, 512], P(('fs', 'rep'), 'tp'), may hold values from -6 to 6
- query_second: float32 [128, 512], P(('fs', 'rep'), 'tp'), may hold values from 0.25 to 4
- value_first: float32 [128, 1024], P(('fs', 'rep'), 'tp'), may hold values from -6 to 6
- value_second: float32 [128, 1024], P(('fs', 'rep'), 'tp'), may hold values from 0.25 to 4
Outputs:
- query_update: float32 [1024, 512], P(('fs', 'rep'), 'tp')
- value_update: float32 [1024, 1024], P(('fs', 'rep'), 'tp')
- query_weight_new: float32 [1024, 512], P(('fs', 'rep'), 'tp')
- value_weight_new: float32 [1024, 1024], P(('fs', 'rep'), 'tp')
- query_first_new: float32 [128, 512], P(('fs', 'rep'), 'tp')
- query_second_new: float32 [128, 512], P(('fs', 'rep'), 'tp')
- value_first_new: float32 [128, 1024], P(('fs', 'rep'), 'tp')
- value_second_new: float32 [128, 1024], P(('fs', 'rep'), 'tp')
- query_copy: bfloat16 [1024, 512], P(None, 'tp')
- value_copy: bfloat16 [1024, 1024], P(None, 'tp')
All inputs are finite; a program needn't handle non-finite values.
Results may differ from a plain program's by a relative error of at most 0.001.
Values may be sent and summed in bfloat16 or wider, within the bound.
A program may use at most 64 MiB of HBM per device.

v0:
```python
import jax
import jax.numpy as jnp
from jax import lax
from jax.sharding import PartitionSpec as P


def cut_along(value, dim, peers):
    before, after = (value.shape[:dim], value.shape[dim + 1 :])
    return jnp.moveaxis(value.reshape(*before, peers, -1, *after), dim, 0)


def summed_on_arrival(value, axis, dim):
    peers = lax.axis_size(axis)
    pieces = lax.all_to_all(cut_along(value, dim, peers), axis, 0, 0, tiled=True)
    return jnp.sum(pieces, axis=0)


def sent_together(arrays, axis, dim, along):
    ends, at = ([], 0)
    for a in arrays[:-1]:
        at += a.shape[along]
        ends.append(at)
    both = jnp.concatenate(arrays, axis=along)
    return tuple(jnp.split(lax.all_gather(both, axis, axis=dim, tiled=True), ends, axis=along))


def sent_to_all(value, axis):
    peers = lax.axis_size(axis)
    return lax.all_to_all(
        jnp.broadcast_to(value[None], (peers, *value.shape)), axis, 0, 0, tiled=True
    )


def over_copies(value, axis):
    return sent_to_all(value, axis).sum(axis=0)


def together(arrays, axis):
    ravelled, at, outs = (jnp.concatenate([a.reshape(-1) for a in arrays]), 0, [])
    total = over_copies(ravelled, axis)
    for a in arrays:
        outs.append(total[at : at + a.size].reshape(a.shape))
        at += a.size
    return tuple(outs)


def moments(projected, first_old, second_old):
    first_new = 0.9 * first_old + 0.1 * projected
    second_new = 0.99 * second_old + 0.01 * projected * projected
    return (first_new, second_new, first_new / (jnp.sqrt(second_new) + 1e-08))


def finish(whole_dir, basis_rows, weight, squares, entries):
    norm_scale = jnp.sqrt(squares / entries + 1.0)
    update = jnp.dot(basis_rows, whole_dir, precision=lax.Precision.HIGHEST) / norm_scale
    weight_new = weight - 0.01 * update
    return (update, weight_new, weight_new.astype(jnp.bfloat16))


def split_parts(reduced):
    high_part = reduced.astype(jnp.bfloat16)
    held = lax.optimization_barrier(high_part)
    low_part = (reduced - held.astype(jnp.float32)).astype(jnp.bfloat16)
    return (high_part, low_part)


def parts_product(high_part, low_part, cotangent):
    dims = (((0,), (0,)), ((), ()))
    first_term = lax.dot_general(high_part, cotangent, dims, preferred_element_type=jnp.float32)
    second_term = lax.dot_general(low_part, cotangent, dims, preferred_element_type=jnp.float32)
    return first_term + second_term


def body(
    normed_input,
    query_cotangent,
    value_cotangent,
    query_basis,
    value_basis,
    query_weight,
    value_weight,
    query_first,
    query_second,
    value_first,
    value_second,
):
    row_count = query_weight.shape[0]
    query_width = query_cotangent.shape[1]
    offset = lax.axis_index(("fs", "rep")) * row_count
    query_rows = lax.dynamic_slice_in_dim(query_basis, offset, row_count, 0).astype(jnp.float32)
    value_rows = lax.dynamic_slice_in_dim(value_basis, offset, row_count, 0).astype(jnp.float32)
    reduced_query = jnp.dot(normed_input, query_basis, preferred_element_type=jnp.float32)
    reduced_value = jnp.dot(normed_input, value_basis, preferred_element_type=jnp.float32)
    query_high, query_low = split_parts(reduced_query)
    value_high, value_low = split_parts(reduced_value)
    projected = summed_on_arrival(
        jnp.concatenate(
            [
                parts_product(query_high, query_low, query_cotangent),
                parts_product(value_high, value_low, value_cotangent),
            ],
            axis=1,
        ),
        ("fs", "rep"),
        0,
    )
    query_projected = projected[:, :query_width]
    value_projected = projected[:, query_width:]
    query_first_new, query_second_new, query_dir = moments(
        query_projected, query_first, query_second
    )
    value_first_new, value_second_new, value_dir = moments(
        value_projected, value_first, value_second
    )
    query_whole, value_whole = sent_together((query_dir, value_dir), ("fs", "rep"), 0, 1)
    query_squares, value_squares = together(
        (jnp.sum(query_whole * query_whole), jnp.sum(value_whole * value_whole)), "tp"
    )
    tp_count = lax.axis_size("tp")
    query_update, query_weight_new, query_half = finish(
        query_whole,
        query_rows,
        query_weight,
        query_squares,
        query_whole.shape[0] * query_whole.shape[1] * tp_count,
    )
    value_update, value_weight_new, value_half = finish(
        value_whole,
        value_rows,
        value_weight,
        value_squares,
        value_whole.shape[0] * value_whole.shape[1] * tp_count,
    )
    query_copy, value_copy = sent_together((query_half, value_half), ("fs", "rep"), 0, 1)
    return (
        query_update,
        value_update,
        query_weight_new,
        value_weight_new,
        query_first_new,
        query_second_new,
        value_first_new,
        value_second_new,
        query_copy,
        value_copy,
    )


def solution(mesh):
    in_specs = (
        P(("fs", "rep"), None),
        P(("fs", "rep"), "tp"),
        P(("fs", "rep"), "tp"),
        P(),
        P(),
        P(("fs", "rep"), "tp"),
        P(("fs", "rep"), "tp"),
        P(("fs", "rep"), "tp"),
        P(("fs", "rep"), "tp"),
        P(("fs", "rep"), "tp"),
        P(("fs", "rep"), "tp"),
    )
    out_specs = (
        P(("fs", "rep"), "tp"),
        P(("fs", "rep"), "tp"),
        P(("fs", "rep"), "tp"),
        P(("fs", "rep"), "tp"),
        P(("fs", "rep"), "tp"),
        P(("fs", "rep"), "tp"),
        P(("fs", "rep"), "tp"),
        P(("fs", "rep"), "tp"),
        P(None, "tp"),
        P(None, "tp"),
    )
    return jax.shard_map(body, mesh=mesh, in_specs=in_specs, out_specs=out_specs, check_vma=False)
```

profile of v0, /device:TPU:2, one launch (start us, length us, event | category | flops | bytes accessed | tf_op | source)
XLA Modules:
  0.0 257.3 jit_solution(1625718977205301110)
XLA Ops:
  0.7 0.9 copy-done
  1.6 1.2 fusion.13
  2.8 0.2 fusion.15
  3.0 0.2 fusion.14
  3.2 0.5 copy-done.3
  3.8 0.2 convolution_add_fusion
  4.3 0.7 reshape.47
  5.1 18.7 %all-to-all-start = ((f32[64,2,192]{2,1,0:T(2,128)}), f32[64,2,192]{2,1,0:T(2,128)S(1)}, u32[]{:S(2)}, u32[]{:S(2)}) async-start(f32[64,2,192]{2,1,0:T(2,128)} %reshape.47), calls=%async_computation | async-start | bytes 262144 | tf_op jit(solution)/shard_map/all_to_all | solution.py:14
  23.8 17.6 %all-to-all-done = f32[64,2,192]{2,1,0:T(2,128)S(1)} async-done(((f32[64,2,192]{2,1,0:T(2,128)}), f32[64,2,192]{2,1,0:T(2,128)S(1)}, u32[]{:S(2)}, u32[]{:S(2)}) %all-to-all-start) | async-done | bytes 98336 | tf_op jit(solution)/shard_map/all_to_all | solution.py:14
  41.6 0.6 add_divide_fusion
  42.3 0.6 add_divide_fusion.1
  42.9 97.2 %all-gather = f32[64,2,192]{2,1,0:T(2,128)S(1)} all-gather(f32[1,2,192]{2,1,0:T(2,128)S(1)} %maximum_bitcast_fusion), channel_id=1, replica_groups=mesh['fs'=16,'rep'=4,'tp'=8] {'fs','rep'}, dimensions={0}, use_global_device_ids=true | all-gather | bytes 99840 | tf_op jit(solution)/shard_map/all_gather | solution.py:24
  140.3 0.7 multiply_reduce_fusion
  140.9 0.6 multiply_reduce_fusion.1
  141.6 1.4 pad_maximum_fusion.2
  142.9 0.6 broadcast_in_dim.2
  143.5 4.8 %all-to-all-start.1 = ((f32[8,1,2]{2,1,0:T(1,128)}), f32[8,1,2]{2,1,0:T(1,128)S(1)}, u32[]{:S(2)}, u32[]{:S(2)}) async-start(f32[8,1,2]{2,1,0:T(1,128)} %broadcast_in_dim.2), calls=%async_computation.1 | async-start | bytes 8192 | tf_op jit(solution)/shard_map/all_to_all | solution.py:29
  148.4 3.8 %all-to-all-done.1 = f32[8,1,2]{2,1,0:T(1,128)S(1)} async-done(((f32[8,1,2]{2,1,0:T(1,128)}), f32[8,1,2]{2,1,0:T(1,128)S(1)}, u32[]{:S(2)}, u32[]{:S(2)}) %all-to-all-start.1) | async-done | bytes 96 | tf_op jit(solution)/shard_map/all_to_all | solution.py:29
  152.1 0.6 fusion.12
  154.2 0.8 fusion.8
  154.9 1.5 fusion.9
  156.5 99.2 %all_gather.7 = bf16[1024,192]{1,0:T(8,128)(2,1)S(1)} all-gather(bf16[16,192]{1,0:T(8,128)(2,1)S(1)} %pad_maximum_fusion.1), channel_id=1, replica_groups=mesh['fs'=16,'rep'=4,'tp'=8] {'fs','rep'}, dimensions={0}, use_global_device_ids=true | all-gather | bytes 399360 | tf_op jit(solution)/shard_map/all_gather | solution.py:24
  255.7 0.8 split.19
  256.5 0.8 copy.30
  (28 shorter events, 0.8 us)
Async XLA Ops:
  0.6 1.0 copy-start
  0.7 2.1 copy-start.2
  0.7 2.3 copy-start.1
  3.0 0.7 copy-start.3
  5.1 36.4 %all-to-all-start = ((f32[64,2,192]{2,1,0:T(2,128)}), f32[64,2,192]{2,1,0:T(2,128)S(1)}, u32[]{:S(2)}, u32[]{:S(2)}) async-start(f32[64,2,192]{2,1,0:T(2,128)} %reshape.47), calls=%async_computation | async-start | bytes 262144 | tf_op jit(solution)/shard_map/all_to_all | solution.py:14
  23.8 17.8 %copy-start.6 = (f32[2,128]{1,0:T(2,128)S(1)}, f32[2,128]{1,0:T(2,128)}, u32[]{:S(2)}) copy-start(f32[2,128]{1,0:T(2,128)} %param.21) | copy-start | bytes 3076
  23.8 17.8 %copy-start.7 = (f32[2,128]{1,0:T(2,128)S(1)}, f32[2,128]{1,0:T(2,128)}, u32[]{:S(2)}) copy-start(f32[2,128]{1,0:T(2,128)} %param.20) | copy-start | bytes 3076
  41.6 0.7 copy-start.8
  41.6 0.7 copy-start.9
  143.5 8.6 %all-to-all-start.1 = ((f32[8,1,2]{2,1,0:T(1,128)}), f32[8,1,2]{2,1,0:T(1,128)S(1)}, u32[]{:S(2)}, u32[]{:S(2)}) async-start(f32[8,1,2]{2,1,0:T(1,128)} %broadcast_in_dim.2), calls=%async_computation.1 | async-start | bytes 8192 | tf_op jit(solution)/shard_map/all_to_all | solution.py:29
  152.7 1.4 copy-start.4
  154.1 0.8 copy-start.5
where the time goes:
time: 258 us; the launch traced here: 257 us
  blocking collectives  196 us (76%)
  starting transfers between devices  23.6 us (9%)
  waiting for transfers between devices  21.4 us (8%)
  local copies, waits for them, and re-layouts  5.24 us (2%)
  matrix products  4.34 us (2%)
  other arithmetic  4.15 us (2%)
    all_gather x2, blocking collectives, sent_together(): lax.all_gather(both, axis, axis=dim, tiled=True)  196 us
    all_to_all x1, starting transfers between devices, summed_on_arrival(): lax.all_to_all(cut_along(value, dim, peers), axis, 0, 0, tiled=True)  18.7 us
    all_to_all x1, waiting for transfers between devices, summed_on_arrival(): lax.all_to_all(cut_along(value, dim, peers), axis, 0, 0, tiled=True)  17.6 us
  transfers between devices with their start and end apart: 2, of which 2 were waited for; matrix products, arithmetic and copies ran while one was open for 0% of the time, Pallas kernels for 0%

commit v1 on v0

v1 whole, which is shorter than its diff:
```python
import functools

import jax
import jax.numpy as jnp
from jax import lax
from jax.experimental import pallas as pl
from jax.experimental.pallas import tpu as pltpu
from jax.sharding import PartitionSpec as P

F32 = jnp.float32
BF16 = jnp.bfloat16
MESH = pl.DeviceIdType.MESH

Z, Y, T = 16, 4, 8
D, RANK = 1024, 128
QL, VL = 64, 128
ROWS = 16
NEAR = (1, -1, 2, -2, 3, -3, 4, -4)
FAR = (8, 7, 9, 6, 10, 5, 11, 4, 12, 3, 13, 2, 14, 1, 15)
SPLIT_GREETING = True


def query_order(p):
    return p >> 6, (p >> 2) & 15, p & 3


def value_order(p):
    return (p >> 2) & 1, p >> 3, p & 3


def rank_of(order, p):
    h, c, i = order(p)
    return 32 * (2 * h + (i >> 1)) + 8 * (c & 3) + 2 * (c >> 2) + (i & 1)


def iota(shape, dim):
    return lax.broadcasted_iota(jnp.int32, shape, dim)


def one_hot(match):
    return jnp.where(match, 1.0, 0.0).astype(F32).astype(BF16)


def nt(a, b):
    return lax.dot_general(a, b, (((1,), (1,)), ((), ())), preferred_element_type=F32)


def nn(a, b):
    return jnp.dot(a, b, preferred_element_type=F32)


def two_parts(value):
    high = value.astype(BF16)
    return high, (value - high.astype(F32)).astype(BF16)


def exchange(
    x_h, cq_h, cv_h, bq_h, bv_h, wq_h, wv_h, fq_h, sq_h, fv_h, sv_h,
    uv_o, uqt_o, uq_o, wv_o, wqt_o, mom_o, tp_o,
    x, cq, cv, bases, wq, wv, olds_q, olds_v,
    gathered, old, part, from_y, chunk, from_z, old_first, old_second, send_ag, from_ag,
    bq2, bv2, dv, dqp, wqn, squares,
    lsem, ysend, yrecv, zsend, zrecv, nsend, nrecv, rsend, rrecv, wsend, wrecv, osend, orecv,
    asend, arecv, tsend, trecv, greet,
):
    z, y, t = lax.axis_index("fs"), lax.axis_index("rep"), lax.axis_index("tp")
    a = lax.rem(z, 4)
    b = lax.div(z, 4)

    def at_z(k):
        return lax.rem(z + (k % Z), Z)

    def at_y(k):
        return lax.rem(y + (k % Y), Y)

    def at_t(k):
        return lax.rem(t + (k % T), T)

    def where(zz, yy, tt):
        return (zz, yy, tt)

    def remote(src, dst, send, recv, device):
        return pltpu.make_async_remote_copy(
            src_ref=src, dst_ref=dst, send_sem=send, recv_sem=recv, device_id=device, device_id_type=MESH
        )

    barrier = pltpu.get_barrier_semaphore()
    met = [where(z, at_y(k), t) for k in (1, 2, 3)] + [where(z, y, at_t(k)) for k in range(1, T)]
    if SPLIT_GREETING:
        met += [where(at_z(k), y, t) for k in (1, 2, -1, -2)]
    else:
        met += [where(at_z(k), y, t) for k in range(1, Z)]
        met += [where(at_z(k), at_y(j), t) for k in (1, 2, -1, -2) for j in (1, 2, 3)]
    for device in met:
        pl.semaphore_signal(barrier, inc=1, device_id=device, device_id_type=MESH)

    loads = [
        (x_h, x), (bq_h, bases.at[:, 0:128]), (bv_h, bases.at[:, 128:256]),
        (cq_h, cq.at[:, 0:128]), (cq_h, cq.at[:, 128:256]),
        (cv_h, cv.at[0:128]), (cv_h, cv.at[128:256]),
        (wq_h, wq), (wv_h, wv),
        (fq_h, olds_q.at[0]), (sq_h, olds_q.at[1]), (fv_h, olds_v.at[0]), (sv_h, olds_v.at[1]),
    ]
    local = [pltpu.make_async_copy(src, dst, lsem.at[n]) for n, (src, dst) in enumerate(loads)]
    for copy in local:
        copy.start()

    for copy in local[7:]:
        copy.wait()
    gathered[0, 4, 0:16] = wv[...]
    gathered[0, 4, 16:24] = jnp.concatenate([wq[0:8], wq[8:16]], axis=1)
    old[b, 0] = olds_v[0]
    old[b, 1] = olds_v[1]
    old[b, 2] = jnp.concatenate([olds_q[0], olds_q[0]], axis=1)
    old[b, 3] = jnp.concatenate([olds_q[1], olds_q[1]], axis=1)

    pending = []

    def send(copy):
        copy.start()
        pending.append(copy)
        return copy

    pl.semaphore_wait(barrier, len(met))

    def near_copy(n):
        k = NEAR[n]
        return remote(gathered.at[0, 4], gathered.at[0, 4 - k], nsend.at[n], nrecv.at[n], where(at_z(k), y, t))

    if SPLIT_GREETING:
        for k in (2, -2):
            pl.semaphore_signal(greet.at[0], inc=1, device_id=where(at_z(k), y, t), device_id_type=MESH)
    for n in range(4):
        send(near_copy(n))

    for copy in local[0:7]:
        copy.wait()
    reduced = nn(x[...], bases[...])
    high, low = two_parts(reduced)
    both = jnp.concatenate([high, low], axis=0)
    p, r = iota((128, 128), 0), iota((128, 128), 1)
    hlq = nt(one_hot(rank_of(query_order, p) == r), both[:, 0:128]).astype(BF16)
    hlv = nt(one_hot(rank_of(value_order, p) == r), both[:, 128:256]).astype(BF16)
    part_q = nt(hlq, cq[...])
    part_v = nn(hlv, cv[...])
    part_q = jnp.concatenate([part_q[0:64], part_q[64:128]], axis=1)
    for j in range(Y):
        part[j, 0:32] = part_v[32 * j : 32 * j + 32]
        part[j, 32:48] = part_q[16 * j : 16 * j + 16]

    def y_copy(k):
        return remote(part.at[at_y(k)], from_y.at[Y - 1 - k], ysend.at[k - 1], yrecv.at[Y - 1 - k], where(z, at_y(k), t))

    for k in (2, 1, 3):
        send(y_copy(k))

    if SPLIT_GREETING:
        pl.semaphore_wait(greet.at[0], 2)
        for k in (4, -4):
            pl.semaphore_signal(greet.at[1], inc=1, device_id=where(at_z(k), y, t), device_id_type=MESH)
    for n in range(4, 8):
        send(near_copy(n))
    if SPLIT_GREETING:
        pl.semaphore_wait(greet.at[1], 2)

    def old_copy(n):
        k = (4, 8, 12)[n]
        return remote(old.at[b], old.at[b], osend.at[n], orecv.at[n], where(at_z(k), y, t))

    for n in range(3):
        send(old_copy(n))

    for k in (1, 2, 3):
        remote(part.at[0], from_y.at[k - 1], ysend.at[k - 1], yrecv.at[k - 1], where(z, y, t)).wait_recv()
    summed = part[y] + from_y[0] + from_y[1] + from_y[2]
    for j in range(4):
        chunk[j, 0] = summed[8 * j : 8 * j + 4]
        chunk[j, 1] = summed[8 * j + 4 : 8 * j + 8]
        chunk[j, 2] = summed[32 + 4 * j : 36 + 4 * j]
    from_z[z] = chunk[a]

    def z_copy(k):
        there = at_z(k)
        return remote(chunk.at[lax.rem(there, 4)], from_z.at[z], zsend.at[k], zrecv.at[k], where(there, y, t))

    for k in FAR:
        send(z_copy(k))

    for n, k in enumerate(NEAR):
        remote(gathered.at[0, 4], gathered.at[0, 4 - k], nsend.at[n], nrecv.at[n], where(z, y, t)).wait_recv()
    relays = [(k, 0) for k in (4, 3, 2, 1)] + [(-k, 8) for k in (3, 2, 1)]
    for n, (k, slot) in enumerate(relays):
        send(remote(gathered.at[0, slot], gathered.at[0, (slot - k) % 16], rsend.at[n], rrecv.at[n], where(at_z(k), y, t)))

    def w_copy(k, piece):
        rows = pl.ds(0, 9) if piece == 0 else pl.ds(9, 7)
        n = 3 * piece + k - 1
        return remote(
            gathered.at[0, rows], gathered.at[Y - k, rows], wsend.at[n], wrecv.at[n], where(z, at_y(k), t)
        )

    for k in (2, 1, 3):
        send(w_copy(k, 0))

    r, p = iota((128, 256), 0), iota((128, 256), 1) & 127
    bq2[...] = nn(bases[:, 0:128], one_hot(rank_of(query_order, p) == r)).astype(BF16)
    bv2[...] = nn(bases[:, 128:256], one_hot(rank_of(value_order, p) == r)).astype(BF16)

    for n in range(3):
        remote(old.at[0], old.at[0], osend.at[n], orecv.at[n], where(z, y, t)).wait_recv()
    left = iota((2, 128), 1) < 64
    for j in range(4):
        h, i = j // 2, 2 * (j % 2)
        mine = left if h == 0 else jnp.logical_not(left)
        old_first[h, i : i + 2] = old[j, 0]
        old_second[h, i : i + 2] = old[j, 1]
        if h == 0:
            old_first[2, i : i + 2] = old[j, 2]
            old_second[2, i : i + 2] = old[j, 3]
        else:
            old_first[2, i : i + 2] = jnp.where(mine, old[j, 2], old_first[2, i : i + 2])
            old_second[2, i : i + 2] = jnp.where(mine, old[j, 3], old_second[2, i : i + 2])

    for k in range(1, Z):
        remote(chunk.at[0], from_z.at[0], zsend.at[k], zrecv.at[k], where(z, y, t)).wait_recv()
    projected = from_z[0]
    for j in range(1, Z):
        projected = projected + from_z[j]
    first_new = 0.9 * old_first[...] + 0.1 * projected
    second_new = 0.99 * old_second[...] + 0.01 * projected * projected
    direction = first_new / (jnp.sqrt(second_new) + 1e-08)
    send_ag[...] = direction
    mom_o[0] = first_new
    mom_o[1] = second_new
    c = 4 * y + a
    from_ag[c] = direction

    targets = [(k, j) for k in (2, 1, -1, 0) for j in (2, 1, 3, 0) if (k, j) != (0, 0)]
    for n, (k, j) in enumerate(targets):
        send(remote(send_ag, from_ag.at[c], asend.at[n], arecv.at[n], where(at_z(k), at_y(j), t)))

    for n, (k, slot) in enumerate(relays):
        remote(gathered.at[0, 0], gathered.at[0, (slot - k) % 16], rsend.at[n], rrecv.at[n], where(z, y, t)).wait_recv()
    for k in (2, 1, 3):
        send(w_copy(k, 1))

    for n in range(len(targets)):
        remote(send_ag, from_ag.at[0], asend.at[n], arecv.at[n], where(z, y, t)).wait_recv()

    square_q, square_v = None, None
    for j in range(16):
        now = from_ag[j]
        q_now = now[2] * now[2]
        v_now = now[0] * now[0] + now[1] * now[1]
        square_q = q_now if square_q is None else square_q + q_now
        square_v = v_now if square_v is None else square_v + v_now
        dv[8 * j : 8 * j + 4] = now[0]
        dv[8 * j + 4 : 8 * j + 8] = now[1]
        dqp[4 * j : 4 * j + 4] = now[2]
    squares[0] = square_q
    squares[1] = square_v
    tp_o[t, 0] = square_q
    tp_o[t, 1] = square_v
    for k in (4, 3, 5, 2, 6, 1, 7):
        send(remote(squares, tp_o.at[t], tsend.at[k], trecv.at[k], where(z, y, at_t(k))))

    vh, vl = two_parts(dv[...])
    uv_o[...] = nn(bv2[...], jnp.concatenate([vh, vl], axis=0))
    turned = jnp.transpose(dqp[...])
    qt = jnp.concatenate([turned[0:64], turned[64:128]], axis=1)
    qh, ql = two_parts(qt)
    qt2 = jnp.concatenate([qh, ql], axis=1)
    uqt_o[...] = nt(qt2, bq2[...])
    own = pl.multiple_of((z * Y + y) * ROWS, ROWS)
    uq_o[...] = nt(bq2[pl.ds(own, ROWS)], qt2)

    for n in range(6):
        piece, k = n // 3, n % 3 + 1
        rows = pl.ds(0, 9) if piece == 0 else pl.ds(9, 7)
        remote(
            gathered.at[0, rows], gathered.at[Y - k, rows], wsend.at[n], wrecv.at[n], where(z, y, t)
        ).wait_recv()

    def place(n, carry):
        slot, dy = lax.div(n, 4), lax.rem(n, 4)
        row = (lax.rem(z + slot + 12, Z) * Y + lax.rem(y + dy, Y)) * ROWS
        row = pl.multiple_of(row, ROWS)
        wv_o[pl.ds(row, 16)] = gathered[dy, slot, 0:16]
        packed = gathered[dy, slot, 16:24]
        wqn[pl.ds(row, 8)] = packed
        wqn[pl.ds(pl.multiple_of(row + 8, 8), 8)] = pltpu.roll(packed, 64, 1)
        return carry

    lax.fori_loop(0, 64, place, 0)
    for j in range(8):
        wqt_o[:, 128 * j : 128 * j + 128] = jnp.transpose(wqn[128 * j : 128 * j + 128])[0:64]

    for k in range(1, T):
        remote(squares, tp_o.at[0], tsend.at[k], trecv.at[k], where(z, y, t)).wait_recv()
    for copy in pending:
        copy.wait_send()


def finish(
    uv, uqt, uq, wv, wqt, mom, tp, wq_own, wv_own,
    uq_o, uv_o, wq_o, wv_o, fq_o, sq_o, fv_o, sv_o, cq_o, cv_o,
):
    z, y = lax.axis_index("fs"), lax.axis_index("rep")
    b = lax.div(z, 4)
    total = tp[0]
    for k in range(1, T):
        total = total + tp[k]
    sum_q = jnp.sum(jnp.sum(total[0], axis=1, keepdims=True), axis=0, keepdims=True)
    sum_v = jnp.sum(jnp.sum(total[1], axis=1, keepdims=True), axis=0, keepdims=True)
    scale_q = 1.0 / jnp.sqrt(sum_q / (RANK * QL * T) + 1.0)
    scale_v = 1.0 / jnp.sqrt(sum_v / (RANK * VL * T) + 1.0)

    cv_o[...] = (wv[...] - 0.01 * (uv[...] * scale_v)).astype(BF16)
    cq_o[...] = (wqt[...] - 0.01 * (uqt[...] * scale_q)).astype(BF16)
    own = pl.multiple_of((z * Y + y) * ROWS, ROWS)
    update_q = uq[...] * scale_q
    update_v = uv[pl.ds(own, ROWS)] * scale_v
    uq_o[...] = update_q
    uv_o[...] = update_v
    wq_o[...] = wq_own[...] - 0.01 * update_q
    wv_o[...] = wv_own[...] - 0.01 * update_v

    for n, (q_out, v_out) in enumerate(((fq_o, fv_o), (sq_o, sv_o))):
        q_rows, v_rows = None, None
        for j in range(4):
            h, i = j // 2, 2 * (j % 2)
            v_now = mom[n, h, i : i + 2]
            q_now = mom[n, 2, i : i + 2, 64 * h : 64 * h + 64]
            q_rows = q_now if q_rows is None else jnp.where(b == j, q_now, q_rows)
            v_rows = v_now if v_rows is None else jnp.where(b == j, v_now, v_rows)
        q_out[...] = q_rows
        v_out[...] = v_rows


def body(x, cq, cv, bq, bv, wq, wv, fq, sq, fv, sv):
    anywhere = pl.BlockSpec(memory_space=pl.ANY)
    inside = pl.BlockSpec(memory_space=pltpu.VMEM)
    shape = jax.ShapeDtypeStruct
    dma = pltpu.SemaphoreType.DMA
    middle = pl.pallas_call(
        exchange,
        out_shape=(
            shape((D, VL), F32), shape((QL, D), F32), shape((ROWS, QL), F32),
            shape((D, VL), F32), shape((QL, D), F32),
            shape((2, 3, 4, 128), F32), shape((T, 2, 4, 128), F32),
        ),
        in_specs=[anywhere] * 11,
        out_specs=[inside] * 7,
        scratch_shapes=[
            pltpu.VMEM((128, D), BF16), pltpu.VMEM((QL, 256), BF16), pltpu.VMEM((256, VL), BF16),
            pltpu.VMEM((D, 256), BF16), pltpu.VMEM((ROWS, QL), F32), pltpu.VMEM((ROWS, VL), F32),
            pltpu.VMEM((2, 2, QL), F32), pltpu.VMEM((2, 2, VL), F32),
            pltpu.VMEM((Y, Z, 24, 128), F32), pltpu.VMEM((4, 4, 2, 128), F32),
            pltpu.VMEM((Y, 48, 128), F32), pltpu.VMEM((Y - 1, 48, 128), F32),
            pltpu.VMEM((4, 3, 4, 128), F32), pltpu.VMEM((Z, 3, 4, 128), F32),
            pltpu.VMEM((3, 4, 128), F32), pltpu.VMEM((3, 4, 128), F32),
            pltpu.VMEM((3, 4, 128), F32), pltpu.VMEM((16, 3, 4, 128), F32),
            pltpu.VMEM((D, 256), BF16), pltpu.VMEM((D, 256), BF16),
            pltpu.VMEM((128, 128), F32), pltpu.VMEM((64, 128), F32),
            pltpu.VMEM((D, 128), F32), pltpu.VMEM((2, 4, 128), F32),
            dma((13,)), dma((3,)), dma((3,)), dma((Z,)), dma((Z,)), dma((8,)), dma((8,)),
            dma((7,)), dma((7,)), dma((6,)), dma((6,)), dma((3,)), dma((3,)),
            dma((15,)), dma((15,)), dma((T,)), dma((T,)),
            pltpu.SemaphoreType.REGULAR((2,)),
        ],
        compiler_params=pltpu.CompilerParams(collective_id=0, has_side_effects=True),
        name="exchange",
    )(x, cq.T, cv, bq, bv, wq, wv, fq, sq, fv, sv)
    outs = pl.pallas_call(
        finish,
        out_shape=(
            shape((ROWS, QL), F32), shape((ROWS, VL), F32), shape((ROWS, QL), F32), shape((ROWS, VL), F32),
            shape((2, QL), F32), shape((2, QL), F32), shape((2, VL), F32), shape((2, VL), F32),
            shape((QL, D), BF16), shape((D, VL), BF16),
        ),
        in_specs=[inside] * 9,
        out_specs=[inside] * 10,
        name="finish",
    )(*middle, wq, wv)
    return (*outs[:8], outs[8].T, outs[9])


def solution(mesh):
    rows = P(("fs", "rep"), "tp")
    in_specs = (P(("fs", "rep"), None), rows, rows, P(), P()) + (rows,) * 6
    out_specs = (rows,) * 8 + (P(None, "tp"),) * 2
    return jax.shard_map(body, mesh=mesh, in_specs=in_specs, out_specs=out_specs, check_vma=False)
```

time: 258 us -> 43.3 us (0.17)
  the two profiles are of different devices: /device:TPU:2 before, /device:TPU:1 now
where the time goes in v1:
time: 43.3 us; the launch traced here: 43 us
  Pallas kernels  42.4 us (98%)
  between operations  0.65 us (2%)
    pallas_call x1, Pallas kernels, body(): pl.pallas_call(exchange, out_shape=(shape((D, VL), F32), shape((QL, D), F...  40 us
    pallas_call x1, Pallas kernels, body(): pl.pallas_call(finish, out_shape=(shape((ROWS, QL), F32), shape((ROWS, VL...  2.37 us

profile of v1, /device:TPU:1, one launch (start us, length us, event | category | flops | bytes accessed | tf_op | source)
XLA Modules:
  0.0 43.0 jit_solution(13429232806916374498)
XLA Ops:
  0.6 40.0 %exchange.1 = (f32[1024,128]{1,0:T(8,128)}, f32[64,1024]{1,0:T(8,128)}, f32[16,64]{1,0:T(8,128)}, f32[1024,128]{1,0:T(8,128)}, f32[64,1024]{1,0:T(8,128)}, /*ind...) custom-call(bf16[128,1024]{1,0:T(8,128)(2,1)} %x_h.1, bf16[64,128]{1,0:T(8,128)(2,1)} %bitcast.2, bf16[128,128]{1,0:T(8,128)(2,1)} %cv_h.1, ...), custom_call_target="tpu_custom_call" | custom-call | tf_op jit(solution)/shard_map/exchange/pallas_call | solution.py:345
  40.6 2.4 %finish.1 = (f32[16,64]{1,0:T(8,128)}, f32[16,128]{1,0:T(8,128)}, f32[16,64]{1,0:T(8,128)}, f32[16,128]{1,0:T(8,128)}, f32[2,64]{1,0:T(2,128)}, /*index=5*/f32[2...) custom-call(f32[1024,128]{1,0:T(8,128)} %get-tuple-element.27.uv, ...), custom_call_target="tpu_custom_call" | custom-call | tf_op jit(solution)/shard_map/finish/pallas_call | solution.py:374

commit v2 on v1

v2 whole, which is shorter than its diff:
```python
import functools

import jax
import jax.numpy as jnp
from jax import lax
from jax.experimental import pallas as pl
from jax.experimental.pallas import tpu as pltpu
from jax.sharding import PartitionSpec as P

F32 = jnp.float32
BF16 = jnp.bfloat16
MESH = pl.DeviceIdType.MESH

Z, Y, T = 16, 4, 8
D, RANK = 1024, 128
QL, VL = 64, 128
ROWS = 16

ROUNDS = ((-2, -1, 0, 1, 2), (-4, -3, 3, 4), (-6, -5, 5, 6), (-7, 7, 8))
SLOT = {rel: n for n, rel in enumerate(sum(ROUNDS, ()))}
STARTS = (0, 5, 9, 13)

PART, CHUNK, DIRECTION, SQUARES, OLD, OLDER, ROUND, WEIGHTS, KINDS = 0, 1, 2, 3, 4, 5, 6, 10, 14


def query_order(p):
    return p >> 6, (p >> 2) & 15, p & 3


def value_order(p):
    return (p >> 2) & 1, p >> 3, p & 3


def rank_of(order, p):
    h, c, i = order(p)
    return 32 * (2 * h + (i >> 1)) + 8 * (c & 3) + 2 * (c >> 2) + (i & 1)


def iota(shape, dim):
    return lax.broadcasted_iota(jnp.int32, shape, dim)


def one_hot(match):
    return jnp.where(match, 1.0, 0.0).astype(F32).astype(BF16)


def nt(a, b):
    return lax.dot_general(a, b, (((1,), (1,)), ((), ())), preferred_element_type=F32)


def nn(a, b):
    return jnp.dot(a, b, preferred_element_type=F32)


def two_parts(value):
    high = value.astype(BF16)
    return high, (value - high.astype(F32)).astype(BF16)


def exchange(
    x_h, cq_h, cv_h, bq_h, bv_h, wq_h, wv_h, fq_h, sq_h, fv_h, sv_h,
    uv_o, uq_o, wv_o, wq_o, mom_o, tp_o,
    x, cq, cv, bases, wq, wv, olds_q, olds_v,
    gathered, old, part, from_y, chunk, from_z, old_first, old_second, send_ag, from_ag,
    bq2, bv2, dv, dqp, squares,
    lsem, sends, recvs, greet,
):
    z, y, t = lax.axis_index("fs"), lax.axis_index("rep"), lax.axis_index("tp")
    a = lax.rem(z, 4)
    b = lax.div(z, 4)

    def at_z(k):
        return lax.rem(z + (k % Z), Z)

    def at_y(k):
        return lax.rem(y + (k % Y), Y)

    def at_t(k):
        return lax.rem(t + (k % T), T)

    def where(zz, yy, tt):
        return (zz, yy, tt)

    def remote(src, dst, kind, device):
        return pltpu.make_async_remote_copy(
            src_ref=src, dst_ref=dst, send_sem=sends.at[kind], recv_sem=recvs.at[kind], device_id=device, device_id_type=MESH
        )

    def arrived(kind, whole):
        remote(whole, whole, kind, where(z, y, t)).wait_recv()

    def left(kind, whole):
        remote(whole, whole, kind, where(z, y, t)).wait_send()

    barrier = pltpu.get_barrier_semaphore()
    met = [where(z, at_y(k), t) for k in (1, 2, 3)] + [where(z, y, at_t(k)) for k in range(1, T)]
    met += [where(at_z(k), y, t) for k in (1, 2, -1, -2)]
    for device in met:
        pl.semaphore_signal(barrier, inc=1, device_id=device, device_id_type=MESH)

    loads = [
        (x_h, x), (bq_h, bases.at[:, 0:128]), (bv_h, bases.at[:, 128:256]),
        (cq_h, cq.at[:, 0:128]), (cq_h, cq.at[:, 128:256]),
        (cv_h, cv.at[0:128]), (cv_h, cv.at[128:256]),
        (wq_h, wq), (wv_h, wv),
        (fq_h, olds_q.at[0]), (sq_h, olds_q.at[1]), (fv_h, olds_v.at[0]), (sv_h, olds_v.at[1]),
    ]
    groups = (0, 1, 1, 2, 2, 3, 3, 4, 5, 6, 6, 7, 7)
    local = [pltpu.make_async_copy(src, dst, lsem.at[groups[n]]) for n, (src, dst) in enumerate(loads)]
    for copy in local:
        copy.start()

    def loaded(group, whole):
        pltpu.make_async_copy(whole, whole, lsem.at[group]).wait()

    loaded(0, x)
    loaded(1, bases)
    reduced = nn(x[...], bases[...])
    high, low = two_parts(reduced)
    both = jnp.concatenate([high, low], axis=0)

    for group, whole in ((2, cq), (3, cv), (4, wq), (5, wv), (6, olds_q), (7, olds_v)):
        loaded(group, whole)
    gathered[0, SLOT[0], 0:16] = wv[...]
    gathered[0, SLOT[0], 16:24] = jnp.concatenate([wq[0:8], wq[8:16]], axis=1)
    old[b, 0] = olds_v[0]
    old[b, 1] = olds_v[1]
    old[b, 2] = jnp.concatenate([olds_q[0], olds_q[1]], axis=1)

    pl.semaphore_wait(barrier, len(met))
    for k in (2, -2):
        pl.semaphore_signal(greet.at[0], inc=1, device_id=where(at_z(k), y, t), device_id_type=MESH)

    def round_copies(level):
        if level == 0:
            moves = [(0, k) for k in (2, -2, 1, -1)]
        else:
            moves = [(-2 * level, 2), (2 * level, -2), (-2 * level, 1), (2 * level, -1)]
        copies = []
        for n, (rel, k) in enumerate(moves):
            there = rel - k
            if there == 8 and k < 0:
                continue
            there = 8 if there == -8 else there
            copies.append(remote(gathered.at[0, SLOT[rel]], gathered.at[0, SLOT[there]], ROUND + level, where(at_z(k), y, t)))
        return copies

    def level_rows(level):
        return pl.ds(STARTS[level], len(ROUNDS[level]))

    def w_copy(k, level):
        rows = level_rows(level)
        return remote(gathered.at[0, rows], gathered.at[Y - k, rows], WEIGHTS + level, where(z, at_y(k), t))

    def go_on(level):
        arrived(ROUND + level, gathered.at[0, pl.ds(0, 3 if level == 3 else 4)])
        if level < 3:
            for copy in round_copies(level + 1):
                copy.start()
        for k in (2, 1, 3):
            w_copy(k, level).start()

    for copy in round_copies(0):
        copy.start()

    p, r = iota((128, 128), 0), iota((128, 128), 1)
    hlq = nt(one_hot(rank_of(query_order, p) == r), both[:, 0:128]).astype(BF16)
    hlv = nt(one_hot(rank_of(value_order, p) == r), both[:, 128:256]).astype(BF16)
    part_q = nt(hlq, cq[...])
    part_v = nn(hlv, cv[...])
    part_q = jnp.concatenate([part_q[0:64], part_q[64:128]], axis=1)
    for j in range(Y):
        part[j, 0:32] = part_v[32 * j : 32 * j + 32]
        part[j, 32:48] = part_q[16 * j : 16 * j + 16]

    def y_copy(k):
        return remote(part.at[at_y(k)], from_y.at[Y - 1 - k], PART, where(z, at_y(k), t))

    for k in (2, 1, 3):
        y_copy(k).start()

    pl.semaphore_wait(greet.at[0], 2)
    for k in (4, -4):
        pl.semaphore_signal(greet.at[1], inc=1, device_id=where(at_z(k), y, t), device_id_type=MESH)

    for k in (4, -4):
        remote(old.at[b], old.at[b], OLD, where(at_z(k), y, t)).start()

    go_on(0)

    arrived(PART, from_y)
    summed = part[y] + from_y[0] + from_y[1] + from_y[2]
    for j in range(4):
        chunk[j, 0] = summed[8 * j : 8 * j + 4]
        chunk[j, 1] = summed[8 * j + 4 : 8 * j + 8]
        chunk[j, 2] = summed[32 + 4 * j : 36 + 4 * j]
    from_z[z] = chunk[a]

    def z_copy(k):
        there = at_z(k)
        return remote(chunk.at[lax.rem(there, 4)], from_z.at[z], CHUNK, where(there, y, t))

    for k in (4, 12, 3, 13, 2, 14, 1, 15):
        z_copy(k).start()

    pl.semaphore_wait(greet.at[1], 2)
    for k in (8, 7, 9, 6, 10, 5, 11):
        z_copy(k).start()

    go_on(1)
    arrived(OLD, old.at[pl.ds(0, 2)])
    before = lax.rem(b + 3, 4)
    remote(old.at[before], old.at[before], OLDER, where(at_z(4), y, t)).start()

    r, p = iota((128, 256), 0), iota((128, 256), 1) & 127
    bq2[...] = nn(bases[:, 0:128], one_hot(rank_of(query_order, p) == r)).astype(BF16)
    bv2[...] = nn(bases[:, 128:256], one_hot(rank_of(value_order, p) == r)).astype(BF16)

    go_on(2)

    arrived(OLDER, old.at[0])
    lower = iota((2, 128), 1) < 64
    for i in (0, 2):
        low_half, high_half = old[i // 2, 2], old[i // 2 + 2, 2]
        for h in range(2):
            old_first[h, i : i + 2] = old[i // 2 + 2 * h, 0]
            old_second[h, i : i + 2] = old[i // 2 + 2 * h, 1]
        old_first[2, i : i + 2] = jnp.where(lower, low_half, pltpu.roll(high_half, 64, 1))
        old_second[2, i : i + 2] = jnp.where(lower, pltpu.roll(low_half, 64, 1), high_half)

    arrived(CHUNK, from_z.at[pl.ds(0, 15)])
    projected = from_z[0]
    for j in range(1, Z):
        projected = projected + from_z[j]
    first_new = 0.9 * old_first[...] + 0.1 * projected
    second_new = 0.99 * old_second[...] + 0.01 * projected * projected
    direction = first_new / (jnp.sqrt(second_new) + 1e-08)
    send_ag[...] = direction
    mom_o[0] = first_new
    mom_o[1] = second_new
    c = 4 * y + a
    from_ag[c] = direction

    targets = [(k, j) for k in (2, 1, -1, 0) for j in (2, 1, 3, 0) if (k, j) != (0, 0)]
    for k, j in targets:
        remote(send_ag, from_ag.at[c], DIRECTION, where(at_z(k), at_y(j), t)).start()

    go_on(3)

    def place(level):
        arrived(WEIGHTS + level, gathered.at[pl.ds(1, 3), level_rows(level)])
        for rel in ROUNDS[level]:
            for dy in range(Y):
                row = (at_z(rel) * Y + at_y(dy)) * ROWS
                row = pl.multiple_of(row, ROWS)
                wv_o[pl.ds(row, 16)] = gathered[dy, SLOT[rel], 0:16]
                packed = gathered[dy, SLOT[rel], 16:24]
                wq_o[pl.ds(row, 8)] = packed
                wq_o[pl.ds(pl.multiple_of(row + 8, 8), 8)] = pltpu.roll(packed, 64, 1)

    place(0)
    place(1)

    arrived(DIRECTION, from_ag.at[pl.ds(0, 15)])

    square_q, square_v = None, None
    for j in range(16):
        now = from_ag[j]
        q_now = now[2] * now[2]
        v_now = now[0] * now[0] + now[1] * now[1]
        square_q = q_now if square_q is None else square_q + q_now
        square_v = v_now if square_v is None else square_v + v_now
        dv[8 * j : 8 * j + 4] = now[0]
        dv[8 * j + 4 : 8 * j + 8] = now[1]
        dqp[4 * j : 4 * j + 4] = now[2]
    squares[0] = square_q
    squares[1] = square_v
    tp_o[t, 0] = square_q
    tp_o[t, 1] = square_v
    for k in (4, 3, 5, 2, 6, 1, 7):
        remote(squares, tp_o.at[t], SQUARES, where(z, y, at_t(k))).start()

    vh, vl = two_parts(dv[...])
    uv_o[...] = nn(bv2[...], jnp.concatenate([vh, vl], axis=0))
    qh, ql = two_parts(jnp.concatenate([dqp[:, 0:64], dqp[:, 64:128]], axis=0))
    uq_o[...] = nn(bq2[...], jnp.concatenate([qh, ql], axis=0))

    place(2)
    place(3)

    arrived(SQUARES, tp_o.at[pl.ds(0, 7)])

    left(PART, from_y)
    left(CHUNK, from_z.at[pl.ds(0, 15)])
    left(DIRECTION, from_ag.at[pl.ds(0, 15)])
    left(SQUARES, tp_o.at[pl.ds(0, 7)])
    left(OLD, old.at[pl.ds(0, 2)])
    left(OLDER, old.at[0])
    for level in range(4):
        left(ROUND + level, gathered.at[0, pl.ds(0, 3 if level == 3 else 4)])
        left(WEIGHTS + level, gathered.at[pl.ds(1, 3), level_rows(level)])


def finish(
    uv, uq, wv, wq, mom, tp,
    uq_o, uv_o, wq_o, wv_o, fq_o, sq_o, fv_o, sv_o, cq_o, cv_o,
):
    z, y = lax.axis_index("fs"), lax.axis_index("rep")
    b = lax.div(z, 4)
    total = tp[0]
    for k in range(1, T):
        total = total + tp[k]
    sum_q = jnp.sum(jnp.sum(total[0], axis=1, keepdims=True), axis=0, keepdims=True)
    sum_v = jnp.sum(jnp.sum(total[1], axis=1, keepdims=True), axis=0, keepdims=True)
    scale_q = 1.0 / jnp.sqrt(sum_q / (RANK * QL * T) + 1.0)
    scale_v = 1.0 / jnp.sqrt(sum_v / (RANK * VL * T) + 1.0)

    half_q = (wq[:, 0:64] - 0.01 * (uq[...] * scale_q)).astype(BF16)
    same = one_hot(iota((QL, QL), 0) == iota((QL, QL), 1))
    cq_o[...] = nt(same, half_q).astype(BF16)
    cv_o[...] = (wv[...] - 0.01 * (uv[...] * scale_v)).astype(BF16)
    own = pl.multiple_of((z * Y + y) * ROWS, ROWS)
    update_q = uq[pl.ds(own, ROWS)] * scale_q
    update_v = uv[pl.ds(own, ROWS)] * scale_v
    uq_o[...] = update_q
    uv_o[...] = update_v
    wq_o[...] = wq[pl.ds(own, ROWS), 0:64] - 0.01 * update_q
    wv_o[...] = wv[pl.ds(own, ROWS)] - 0.01 * update_v

    for n, (q_out, v_out) in enumerate(((fq_o, fv_o), (sq_o, sv_o))):
        q_rows, v_rows = None, None
        for j in range(4):
            h, i = j // 2, 2 * (j % 2)
            v_now = mom[n, h, i : i + 2]
            q_now = mom[n, 2, i : i + 2, 64 * h : 64 * h + 64]
            q_rows = q_now if q_rows is None else jnp.where(b == j, q_now, q_rows)
            v_rows = v_now if v_rows is None else jnp.where(b == j, v_now, v_rows)
        q_out[...] = q_rows
        v_out[...] = v_rows


def body(x, cq, cv, bq, bv, wq, wv, fq, sq, fv, sv):
    anywhere = pl.BlockSpec(memory_space=pltpu.HBM)
    inside = pl.BlockSpec(memory_space=pltpu.VMEM)
    shape = jax.ShapeDtypeStruct
    dma = pltpu.SemaphoreType.DMA
    middle = pl.pallas_call(
        exchange,
        out_shape=(
            shape((D, VL), F32), shape((D, QL), F32), shape((D, VL), F32), shape((D, 128), F32),
            shape((2, 3, 4, 128), F32), shape((T, 2, 4, 128), F32),
        ),
        in_specs=[anywhere] * 11,
        out_specs=[inside] * 6,
        scratch_shapes=[
            pltpu.VMEM((128, D), BF16), pltpu.VMEM((QL, 256), BF16), pltpu.VMEM((256, VL), BF16),
            pltpu.VMEM((D, 256), BF16), pltpu.VMEM((ROWS, QL), F32), pltpu.VMEM((ROWS, VL), F32),
            pltpu.VMEM((2, 2, QL), F32), pltpu.VMEM((2, 2, VL), F32),
            pltpu.VMEM((Y, Z, 24, 128), F32), pltpu.VMEM((4, 3, 2, 128), F32),
            pltpu.VMEM((Y, 48, 128), F32), pltpu.VMEM((Y - 1, 48, 128), F32),
            pltpu.VMEM((4, 3, 4, 128), F32), pltpu.VMEM((Z, 3, 4, 128), F32),
            pltpu.VMEM((3, 4, 128), F32), pltpu.VMEM((3, 4, 128), F32),
            pltpu.VMEM((3, 4, 128), F32), pltpu.VMEM((16, 3, 4, 128), F32),
            pltpu.VMEM((D, 256), BF16), pltpu.VMEM((D, 256), BF16),
            pltpu.VMEM((128, 128), F32), pltpu.VMEM((64, 128), F32),
            pltpu.VMEM((2, 4, 128), F32),
            dma((8,)), dma((KINDS,)), dma((KINDS,)),
            pltpu.SemaphoreType.REGULAR((2,)),
        ],
        compiler_params=pltpu.CompilerParams(collective_id=0, has_side_effects=True, vmem_limit_bytes=12 << 20),
        name="exchange",
    )(*(pltpu.with_memory_space_constraint(a, pltpu.HBM) for a in (x, cq.T, cv, bq, bv, wq, wv, fq, sq, fv, sv)))
    outs = pl.pallas_call(
        finish,
        out_shape=(
            shape((ROWS, QL), F32), shape((ROWS, VL), F32), shape((ROWS, QL), F32), shape((ROWS, VL), F32),
            shape((2, QL), F32), shape((2, QL), F32), shape((2, VL), F32), shape((2, VL), F32),
            shape((QL, D), BF16), shape((D, VL), BF16),
        ),
        in_specs=[inside] * 6,
        out_specs=[inside] * 10,
        compiler_params=pltpu.CompilerParams(vmem_limit_bytes=12 << 20),
        name="finish",
    )(*middle)
    return (*outs[:8], outs[8].T, outs[9])


def solution(mesh):
    rows = P(("fs", "rep"), "tp")
    in_specs = (P(("fs", "rep"), None), rows, rows, P(), P()) + (rows,) * 6
    out_specs = (rows,) * 8 + (P(None, "tp"),) * 2
    return jax.shard_map(body, mesh=mesh, in_specs=in_specs, out_specs=out_specs, check_vma=False)
```

time: 43.3 us -> 38.3 us (0.88)
  Pallas kernels: 42.4 us -> 37.5 us
    pallas_call x1, Pallas kernels: 40 us -> 36.4 us  [body(): pl.pallas_call(exchange, out_shape=(shape((D, VL), F32), shape((D, QL), F...]
    pallas_call x1, Pallas kernels: 2.37 us -> 1.11 us  [body(): pl.pallas_call(finish, out_shape=(shape((ROWS, QL), F32), shape((ROWS, VL...]
where the time goes in v2:
time: 38.3 us; the launch traced here: 38.2 us
  Pallas kernels  37.5 us (98%)
  between operations  0.65 us (2%)
    pallas_call x1, Pallas kernels, body(): pl.pallas_call(exchange, out_shape=(shape((D, VL), F32), shape((D, QL), F...  36.4 us
    pallas_call x1, Pallas kernels, body(): pl.pallas_call(finish, out_shape=(shape((ROWS, QL), F32), shape((ROWS, VL...  1.11 us

profile of v2, /device:TPU:1, one launch (start us, length us, event | category | flops | bytes accessed | tf_op | source)
XLA Modules:
  0.0 38.2 jit_solution(11253851840851850570)
XLA Ops:
  0.6 36.4 %exchange.1 = (f32[1024,128]{1,0:T(8,128)S(1)}, f32[1024,64]{1,0:T(8,128)S(1)}, f32[1024,128]{1,0:T(8,128)S(1)}, f32[1024,128]{1,0:T(8,128)S(1)}, f32[2,3,4,128]...) custom-call(bf16[128,1024]{1,0:T(8,128)(2,1)} %x_h.1, bf16[64,128]{1,0:T(8,128)(2,1)} %bitcast.2, bf16[128,128]{1,0:T(8,128)(2,1)} %cv_h.1, ...), custom_call_target="tpu_custom_call" | custom-call | tf_op jit(solution)/shard_map/exchange/pallas_call | solution.py:347
  37.1 1.1 %finish.1 = (f32[16,64]{1,0:T(8,128)}, f32[16,128]{1,0:T(8,128)}, f32[16,64]{1,0:T(8,128)}, f32[16,128]{1,0:T(8,128)}, f32[2,64]{1,0:T(2,128)}, /*index=5*/f32[2...) custom-call(f32[1024,128]{1,0:T(8,128)S(1)} %get-tuple-element.26.uv, ...), custom_call_target="tpu_custom_call" | custom-call | tf_op jit(solution)/shard_map/finish/pallas_call | solution.py:373

commit v3 on v2

v3 whole, which is shorter than its diff:
```python
import functools

import jax
import jax.numpy as jnp
from jax import lax
from jax.experimental import pallas as pl
from jax.experimental.pallas import tpu as pltpu
from jax.sharding import PartitionSpec as P

F32 = jnp.float32
BF16 = jnp.bfloat16
MESH = pl.DeviceIdType.MESH

Z, Y, T, X = 16, 4, 8, 4
D, RANK = 1024, 128
QL, VL = 64, 128
ROWS = 16

ROUNDS = ((-3, -2, -1, 0, 1, 2, 3), (-6, -5, -4, 4, 5, 6), (-7, 7, 8))
SLOT = {rel: n for n, rel in enumerate(sum(ROUNDS, ()))}
STARTS = (0, 7, 13)
MOVES = (
    ((0, 3, -3), (0, -3, 3), (0, 2, -2), (0, -2, 2), (0, 1, -1), (0, -1, 1)),
    ((-3, 3, -6), (3, -3, 6), (-3, 2, -5), (3, -2, 5), (-3, 1, -4), (3, -1, 4)),
    ((-6, 2, 8), (-6, 1, -7), (6, -1, 7)),
)

PART, CHUNK, DIRECTION, DIRECTION_0, SQUARES, MOMENTS, OWN_OLD, OLD, OLDER = range(9)
ROUND, WEIGHTS, KINDS = 9, 12, 15


def query_order(p):
    return p >> 6, (p >> 2) & 15, p & 3


def value_order(p):
    return (p >> 2) & 1, p >> 3, p & 3


def rank_of(order, p):
    h, c, i = order(p)
    a = 2 * (c & 1) + ((c >> 1) & 1)
    return 32 * (2 * h + (i >> 1)) + 8 * a + 2 * (c >> 2) + (i & 1)


def iota(shape, dim):
    return lax.broadcasted_iota(jnp.int32, shape, dim)


def one_hot(match):
    return jnp.where(match, 1.0, 0.0).astype(F32).astype(BF16)


def nt(a, b):
    return lax.dot_general(a, b, (((1,), (1,)), ((), ())), preferred_element_type=F32)


def nn(a, b):
    return jnp.dot(a, b, preferred_element_type=F32)


def two_parts(value):
    high = value.astype(BF16)
    return high, (value - high.astype(F32)).astype(BF16)


def exchange(
    x_h, cq_h, cv_h, bq_h, bv_h, wq_h, wv_h, fq_h, sq_h, fv_h, sv_h,
    uv_o, uq_o, wv_o, wq_o, mom_o, squares_o,
    x, cq, cv, bases, wq, wv, olds_q, olds_v,
    gathered, own_old, old, part, from_y, chunk, from_z, old_first, old_second, send_ag, from_ag,
    bq2, bv2, dv, dqp, square, room,
    lsem, sends, recvs, greet,
):
    z, y, t = lax.axis_index("fs"), lax.axis_index("rep"), lax.axis_index("tp")
    a = lax.rem(z, 4)
    b = lax.div(z, 4)
    xi = lax.div(t, 2)
    core = lax.rem(t, 2)
    t0, t1 = 2 * xi, 2 * xi + 1
    c = 4 * y + 2 * lax.rem(a, 2) + lax.div(a, 2)
    odd = lax.rem(z, 2)
    pair, mate = lax.div(z, 2), z + 1 - 2 * odd

    def at_z(k):
        return lax.rem(z + (k % Z), Z)

    def at_y(k):
        return lax.rem(y + (k % Y), Y)

    def at_x(k, core_there):
        return 2 * lax.rem(xi + (k % X), X) + core_there

    def remote(src, dst, kind, device):
        return pltpu.make_async_remote_copy(
            src_ref=src, dst_ref=dst, send_sem=sends.at[kind], recv_sem=recvs.at[kind], device_id=device, device_id_type=MESH
        )

    def arrived(kind, whole):
        remote(whole, whole, kind, (z, y, t)).wait_recv()

    def left(kind, whole):
        remote(whole, whole, kind, (z, y, t)).wait_send()

    def hello(semaphore, device):
        pl.semaphore_signal(semaphore, inc=1, device_id=device, device_id_type=MESH)

    barrier = pltpu.get_barrier_semaphore()
    for k in range(Y):
        @pl.when(core == 1)
        def _():
            hello(barrier, (z, at_y(k), t0))
            hello(barrier, (mate, at_y(k), t0))
            if k:
                hello(barrier, (z, at_y(k), t1))
                hello(barrier, (mate, at_y(k), t1))

        @pl.when(core == 0)
        def _():
            hello(barrier, (z, at_y(k), t1))

            if k:
                hello(barrier, (z, at_y(k), t0))

    for k in (3, -3, 2, -2, 1, -1):
        hello(barrier, (at_z(k), y, t))
    for k in range(1, X):
        hello(barrier, (z, y, at_x(k, 1)))

    loads = [
        (x_h, x), (bq_h, bases.at[:, 0:128]), (bv_h, bases.at[:, 128:256]),
        (cq_h, cq.at[:, 0:128]), (cq_h, cq.at[:, 128:256]),
        (cv_h, cv.at[0:128]), (cv_h, cv.at[128:256]),
        (wq_h, wq), (wv_h, wv),
        (fq_h, olds_q.at[0]), (sq_h, olds_q.at[1]), (fv_h, olds_v.at[0]), (sv_h, olds_v.at[1]),
    ]
    groups = (0, 1, 1, 2, 2, 3, 3, 4, 5, 6, 6, 7, 7)
    for n, (src, dst) in enumerate(loads):
        pltpu.make_async_copy(src, dst, lsem.at[groups[n]]).start()

    def loaded(group, whole):
        pltpu.make_async_copy(whole, whole, lsem.at[group]).wait()

    loaded(0, x)
    loaded(1, bases)
    reduced = nn(x[...], bases[...])
    high, low = two_parts(reduced)
    both = jnp.concatenate([high, low], axis=0)

    for group, whole in ((2, cq), (3, cv), (4, wq), (5, wv), (6, olds_q), (7, olds_v)):
        loaded(group, whole)
    gathered[0, SLOT[0], 0:16] = wv[...]
    gathered[0, SLOT[0], 16:24] = jnp.concatenate([wq[0:8], wq[8:16]], axis=1)
    own_old[0] = olds_v[0]
    own_old[1] = olds_v[1]
    own_old[2] = jnp.concatenate([olds_q[0], olds_q[1]], axis=1)

    def round_copies(level):
        for rel, k, there in MOVES[level]:
            remote(gathered.at[0, SLOT[rel]], gathered.at[0, SLOT[there]], ROUND + level, (at_z(k), y, t)).start()

    def level_rows(level):
        return pl.ds(STARTS[level], len(ROUNDS[level]))

    def round_wait_shape(level):
        return gathered.at[0, pl.ds(0, len(MOVES[level]))]

    def go_on(level):
        arrived(ROUND + level, round_wait_shape(level))
        if level < 2:
            round_copies(level + 1)
        rows = level_rows(level)
        for k in (2, 1, 3):
            remote(gathered.at[0, rows], gathered.at[Y - k, rows], WEIGHTS + level, (z, at_y(k), t)).start()

    p, r = iota((128, 128), 0), iota((128, 128), 1)
    hlq = nt(one_hot(rank_of(query_order, p) == r), both[:, 0:128]).astype(BF16)
    hlv = nt(one_hot(rank_of(value_order, p) == r), both[:, 128:256]).astype(BF16)
    part_q = nt(hlq, cq[...])
    part_v = nn(hlv, cv[...])
    part_q = jnp.concatenate([part_q[0:64], part_q[64:128]], axis=1)
    for j in range(Y):
        for n in range(2):
            m = 2 * j + n
            part[j, n, 0:16] = part_v[16 * m : 16 * m + 16]
            part[j, n, 16:24] = part_q[8 * m : 8 * m + 8]

    @pl.when(core == 1)
    def _():
        pl.semaphore_wait(barrier, 22)
        for k in (3, -3):
            hello(greet.at[0], (at_z(k), y, t))

    @pl.when(core == 0)
    def _():
        pl.semaphore_wait(barrier, 17)
        remote(own_old, old.at[b, 0], OWN_OLD, (z, y, t1)).start()

    def part_copy(n, k):
        slot = 2 * (Y * n + (Y - k) % Y) + core
        there, parity = (mate, 1 - odd) if n else (z, odd)
        remote(part.at[at_y(k), parity], from_y.at[slot], PART, (there, at_y(k), t1)).start()

    for k in (2, 1, 3, 0):
        for n in (1, 0):
            if n or k:
                part_copy(n, k)

    @pl.when(core == 0)
    def _():
        part_copy(0, 0)

    round_copies(0)

    def permuted_bases():
        r, p = iota((128, 256), 0), iota((128, 256), 1) & 127
        bq2[...] = nn(bases[:, 0:128], one_hot(rank_of(query_order, p) == r)).astype(BF16)
        bv2[...] = nn(bases[:, 128:256], one_hot(rank_of(value_order, p) == r)).astype(BF16)

    def place(level):
        arrived(WEIGHTS + level, gathered.at[pl.ds(1, 3), level_rows(level)])
        for rel in ROUNDS[level]:
            for dy in range(Y):
                row = (at_z(rel) * Y + at_y(dy)) * ROWS
                row = pl.multiple_of(row, ROWS)
                wv_o[pl.ds(row, 16)] = gathered[dy, SLOT[rel], 0:16]
                packed = gathered[dy, SLOT[rel], 16:24]
                wq_o[pl.ds(row, 8)] = packed
                wq_o[pl.ds(pl.multiple_of(row + 8, 8), 8)] = pltpu.roll(packed, 64, 1)

    def weights_left():
        for level in range(3):
            left(ROUND + level, round_wait_shape(level))
            left(WEIGHTS + level, gathered.at[pl.ds(1, 3), level_rows(level)])

    def updates():
        for j in range(16):
            dv[8 * j : 8 * j + 4] = from_ag[j, 0]
            dv[8 * j + 4 : 8 * j + 8] = from_ag[j, 1]
            dqp[4 * j : 4 * j + 4] = from_ag[j, 2]
        vh, vl = two_parts(dv[...])
        uv_o[...] = nn(bv2[...], jnp.concatenate([vh, vl], axis=0))
        qh, ql = two_parts(jnp.concatenate([dqp[:, 0:64], dqp[:, 64:128]], axis=0))
        uq_o[...] = nn(bq2[...], jnp.concatenate([qh, ql], axis=0))

    @pl.when(core == 0)
    def _():
        permuted_bases()
        go_on(0)
        go_on(1)
        place(0)
        go_on(2)
        place(1)
        arrived(DIRECTION_0, from_ag)
        updates()
        place(2)
        arrived(SQUARES, squares_o)
        arrived(MOMENTS, mom_o)
        left(OWN_OLD, own_old)
        left(PART, from_y.at[pl.ds(0, 8)])
        weights_left()

    @pl.when(core == 1)
    def _():
        old[b, 1] = own_old[...]
        arrived(OWN_OLD, own_old)
        pl.semaphore_wait(greet.at[0], 2)
        for k in (2, -2):
            hello(greet.at[1], (at_z(k), y, t))
        for k in (4, -4):
            remote(old.at[b], old.at[b], OLD, (at_z(k), y, t)).start()
        arrived(PART, from_y.at[pl.ds(0, 15)])
        summed = [from_y[0], part[y, odd]]
        for j in range(1, 2 * Y):
            summed = [summed[0] + from_y[2 * j], summed[1] + from_y[2 * j + 1]]
        for j in range(2):
            for n, now in enumerate(summed):
                chunk[j, 3 * n] = now[8 * j : 8 * j + 4]
                chunk[j, 3 * n + 1] = now[8 * j + 4 : 8 * j + 8]
                chunk[j, 3 * n + 2] = now[16 + 4 * j : 20 + 4 * j]
        from_z[pair] = chunk[lax.rem(pair, 2)]

        def z_copy(k):
            there = at_z(k)
            remote(chunk.at[lax.rem(lax.div(there, 2), 2)], from_z.at[pair], CHUNK, (there, y, t)).start()

        for k in (6, 10):
            z_copy(k)

        pl.semaphore_wait(greet.at[1], 2)
        for k in (8, 4, 12, 2, 14):
            z_copy(k)


        go_on(0)

        arrived(OLD, old.at[pl.ds(0, 2)])
        before = lax.rem(b + 3, 4)
        remote(old.at[before], old.at[before], OLDER, (at_z(4), y, t)).start()

        go_on(1)

        permuted_bases()

        arrived(OLDER, old.at[0])
        lower = iota((2, 128), 1) < 64
        for n in range(2):
            for i in (0, 2):
                low_half, high_half = old[i // 2, n, 2], old[i // 2 + 2, n, 2]
                for h in range(2):
                    old_first[3 * n + h, i : i + 2] = old[i // 2 + 2 * h, n, 0]
                    old_second[3 * n + h, i : i + 2] = old[i // 2 + 2 * h, n, 1]
                old_first[3 * n + 2, i : i + 2] = jnp.where(lower, low_half, pltpu.roll(high_half, 64, 1))
                old_second[3 * n + 2, i : i + 2] = jnp.where(lower, pltpu.roll(low_half, 64, 1), high_half)

        arrived(CHUNK, from_z.at[pl.ds(0, 7)])
        projected = from_z[0]
        for j in range(1, Z // 2):
            projected = projected + from_z[j]
        first_new = 0.9 * old_first[...] + 0.1 * projected
        second_new = 0.99 * old_second[...] + 0.01 * projected * projected
        direction = first_new / (jnp.sqrt(second_new) + 1e-08)
        send_ag[0] = direction
        squared = direction * direction
        square_q = squared[2] + squared[5]
        square_v = squared[0] + squared[1] + squared[3] + squared[4]
        square_q = jnp.sum(square_q, axis=0, keepdims=True)
        square_v = jnp.sum(square_v, axis=0, keepdims=True)
        square_q = square_q + pltpu.roll(square_q, 64, 1)
        square_v = square_v + pltpu.roll(square_v, 64, 1)
        row = jnp.where(iota((1, 128), 1) < 64, square_q, square_v)
        square[...] = row
        there = 16 * xi + c
        def send_squares(dxs):
            for dx in dxs:
                for k in (2, 1, -1, 0):
                    for j in (2, 1, 3, 0):
                        for n in range(2):
                            if (dx, k, j, n) != (0, 0, 0, 1):
                                remote(square, squares_o.at[there], SQUARES, (at_z(k), at_y(j), at_x(dx, n))).start()

        send_squares((2, 1, 3))
        for k in (2, 1, -1, 0):
            for j in (2, 1, 3, 0):
                remote(send_ag.at[0, pl.ds(0, 3)], from_ag.at[c], DIRECTION_0, (at_z(k), at_y(j), t0)).start()
                if (k, j) != (0, 0):
                    remote(send_ag.at[0, pl.ds(3, 3)], from_ag.at[c], DIRECTION, (at_z(k), at_y(j), t)).start()
        send_squares((0,))
        squares_o[there] = row
        from_ag[c] = direction[3:6]
        send_ag[1] = first_new
        send_ag[2] = second_new
        mom_o[0] = first_new[3:6]
        mom_o[1] = second_new[3:6]
        remote(send_ag.at[pl.ds(1, 2), pl.ds(0, 3)], mom_o, MOMENTS, (z, y, t0)).start()

        go_on(2)

        place(0)
        place(1)

        arrived(DIRECTION, from_ag.at[pl.ds(0, 15)])
        updates()
        place(2)

        arrived(SQUARES, squares_o.at[pl.ds(0, 63)])

        left(PART, from_y.at[pl.ds(0, 7)])
        left(CHUNK, from_z.at[pl.ds(0, 7)])
        left(DIRECTION, from_ag.at[pl.ds(0, 15)])
        left(DIRECTION_0, from_ag)
        left(MOMENTS, mom_o)
        left(OLD, old.at[pl.ds(0, 2)])
        left(OLDER, old.at[0])
        weights_left()
        left(SQUARES, room)


def finish(
    uv, uq, wv, wq, mom, squares,
    uq_o, uv_o, wq_o, wv_o, fq_o, sq_o, fv_o, sv_o, cq_o, cv_o,
):
    z, y = lax.axis_index("fs"), lax.axis_index("rep")
    b = lax.div(z, 4)
    total = squares[0]
    for k in range(1, 16 * X):
        total = total + squares[k]
    query_lanes = iota((1, 128), 1) < 64
    sum_q = jnp.sum(jnp.where(query_lanes, total, 0.0), axis=1, keepdims=True)
    sum_v = jnp.sum(jnp.where(query_lanes, 0.0, total), axis=1, keepdims=True)
    scale_q = 1.0 / jnp.sqrt(sum_q / (RANK * QL * T) + 1.0)
    scale_v = 1.0 / jnp.sqrt(sum_v / (RANK * VL * T) + 1.0)

    half_q = (wq[:, 0:64] - 0.01 * (uq[...] * scale_q)).astype(BF16)
    same = one_hot(iota((QL, QL), 0) == iota((QL, QL), 1))
    cq_o[...] = nt(same, half_q).astype(BF16)
    cv_o[...] = (wv[...] - 0.01 * (uv[...] * scale_v)).astype(BF16)
    own = pl.multiple_of((z * Y + y) * ROWS, ROWS)
    update_q = uq[pl.ds(own, ROWS)] * scale_q
    update_v = uv[pl.ds(own, ROWS)] * scale_v
    uq_o[...] = update_q
    uv_o[...] = update_v
    wq_o[...] = wq[pl.ds(own, ROWS), 0:64] - 0.01 * update_q
    wv_o[...] = wv[pl.ds(own, ROWS)] - 0.01 * update_v

    for n, (q_out, v_out) in enumerate(((fq_o, fv_o), (sq_o, sv_o))):
        q_rows, v_rows = None, None
        for j in range(4):
            h, i = j // 2, 2 * (j % 2)
            v_now = mom[n, h, i : i + 2]
            q_now = mom[n, 2, i : i + 2, 64 * h : 64 * h + 64]
            q_rows = q_now if q_rows is None else jnp.where(b == j, q_now, q_rows)
            v_rows = v_now if v_rows is None else jnp.where(b == j, v_now, v_rows)
        q_out[...] = q_rows
        v_out[...] = v_rows


def body(x, cq, cv, bq, bv, wq, wv, fq, sq, fv, sv):
    anywhere = pl.BlockSpec(memory_space=pltpu.HBM)
    inside = pl.BlockSpec(memory_space=pltpu.VMEM)
    shape = jax.ShapeDtypeStruct
    dma = pltpu.SemaphoreType.DMA
    middle = pl.pallas_call(
        exchange,
        out_shape=(
            shape((D, VL), F32), shape((D, QL), F32), shape((D, VL), F32), shape((D, 128), F32),
            shape((2, 3, 4, 128), F32), shape((16 * X, 1, 128), F32),
        ),
        in_specs=[anywhere] * 11,
        out_specs=[inside] * 6,
        scratch_shapes=[
            pltpu.VMEM((128, D), BF16), pltpu.VMEM((QL, 256), BF16), pltpu.VMEM((256, VL), BF16),
            pltpu.VMEM((D, 256), BF16), pltpu.VMEM((ROWS, QL), F32), pltpu.VMEM((ROWS, VL), F32),
            pltpu.VMEM((2, 2, QL), F32), pltpu.VMEM((2, 2, VL), F32),
            pltpu.VMEM((Y, Z, 24, 128), F32),
            pltpu.VMEM((3, 2, 128), F32), pltpu.VMEM((4, 2, 3, 2, 128), F32),
            pltpu.VMEM((Y, 2, 24, 128), F32), pltpu.VMEM((4 * Y, 24, 128), F32),
            pltpu.VMEM((2, 6, 4, 128), F32), pltpu.VMEM((Z // 2, 6, 4, 128), F32),
            pltpu.VMEM((6, 4, 128), F32), pltpu.VMEM((6, 4, 128), F32),
            pltpu.VMEM((3, 6, 4, 128), F32), pltpu.VMEM((16, 3, 4, 128), F32),
            pltpu.VMEM((D, 256), BF16), pltpu.VMEM((D, 256), BF16),
            pltpu.VMEM((128, 128), F32), pltpu.VMEM((64, 128), F32), pltpu.VMEM((1, 128), F32),
            pltpu.VMEM((127, 1, 128), F32),
            dma((8,)), dma((KINDS,)), dma((KINDS,)),
            pltpu.SemaphoreType.REGULAR((2,)),
        ],
        compiler_params=pltpu.CompilerParams(collective_id=0, has_side_effects=True, vmem_limit_bytes=12 << 20),
        name="exchange",
    )(*(pltpu.with_memory_space_constraint(a, pltpu.HBM) for a in (x, cq.T, cv, bq, bv, wq, wv, fq, sq, fv, sv)))
    outs = pl.pallas_call(
        finish,
        out_shape=(
            shape((ROWS, QL), F32), shape((ROWS, VL), F32), shape((ROWS, QL), F32), shape((ROWS, VL), F32),
            shape((2, QL), F32), shape((2, QL), F32), shape((2, VL), F32), shape((2, VL), F32),
            shape((QL, D), BF16), shape((D, VL), BF16),
        ),
        in_specs=[inside] * 6,
        out_specs=[inside] * 10,
        compiler_params=pltpu.CompilerParams(vmem_limit_bytes=12 << 20),
        name="finish",
    )(*middle)
    return (*outs[:8], outs[8].T, outs[9])


def solution(mesh):
    rows = P(("fs", "rep"), "tp")
    in_specs = (P(("fs", "rep"), None), rows, rows, P(), P()) + (rows,) * 6
    out_specs = (rows,) * 8 + (P(None, "tp"),) * 2
    return jax.shard_map(body, mesh=mesh, in_specs=in_specs, out_specs=out_specs, check_vma=False)
```

time: 38.3 us -> 35.2 us (0.919)
  Pallas kernels: 37.5 us -> 34.4 us
    pallas_call x1, Pallas kernels: 36.4 us -> 33.2 us  [body(): pl.pallas_call(exchange, out_shape=(shape((D, VL), F32), shape((D, QL), F...]
where the time goes in v3:
time: 35.2 us; the launch traced here: 35 us
  Pallas kernels  34.4 us (98%)
  between operations  0.65 us (2%)
    pallas_call x1, Pallas kernels, body(): pl.pallas_call(exchange, out_shape=(shape((D, VL), F32), shape((D, QL), F...  33.2 us
    pallas_call x1, Pallas kernels, body(): pl.pallas_call(finish, out_shape=(shape((ROWS, QL), F32), shape((ROWS, VL...  1.16 us

profile of v3, /device:TPU:1, one launch (start us, length us, event | category | flops | bytes accessed | tf_op | source)
XLA Modules:
  0.0 35.0 jit_solution(14403006549159171800)
XLA Ops:
  0.6 33.2 %exchange.1 = (f32[1024,128]{1,0:T(8,128)S(1)}, f32[1024,64]{1,0:T(8,128)S(1)}, f32[1024,128]{1,0:T(8,128)S(1)}, f32[1024,128]{1,0:T(8,128)S(1)}, f32[2,3,4,128]...) custom-call(bf16[128,1024]{1,0:T(8,128)(2,1)} %x_h.1, bf16[64,128]{1,0:T(8,128)(2,1)} %bitcast.2, bf16[128,128]{1,0:T(8,128)(2,1)} %cv_h.1, ...), custom_call_target="tpu_custom_call" | custom-call | tf_op jit(solution)/shard_map/exchange/pallas_call | solution.py:423
  33.9 1.2 %finish.1 = (f32[16,64]{1,0:T(8,128)}, f32[16,128]{1,0:T(8,128)}, f32[16,64]{1,0:T(8,128)}, f32[16,128]{1,0:T(8,128)}, f32[2,64]{1,0:T(2,128)}, /*index=5*/f32[2...) custom-call(f32[1024,128]{1,0:T(8,128)S(1)} %get-tuple-element.26.uv, ...), custom_call_target="tpu_custom_call" | custom-call | tf_op jit(solution)/shard_map/finish/pallas_call | solution.py:450

commit v4 on v3

--- a/solution.py
+++ b/solution.py
@@ -1,5 +1,3 @@
-import functools
-
 import jax
 import jax.numpy as jnp
 from jax import lax
@@ -25,8 +23,8 @@
     ((-6, 2, 8), (-6, 1, -7), (6, -1, 7)),
 )
 
-PART, CHUNK, DIRECTION, DIRECTION_0, SQUARES, MOMENTS, OWN_OLD, OLD, OLDER = range(9)
-ROUND, WEIGHTS, KINDS = 9, 12, 15
+PART, CHUNK, DIRECTION, DIRECTION_0, SQUARES, MOMENTS, OWN_OLD, OLD = range(8)
+ROUND, WEIGHTS, KINDS = 8, 11, 14
 
 
 def query_order(p):
@@ -167,11 +165,13 @@
 
     def go_on(level):
         arrived(ROUND + level, round_wait_shape(level))
-        if level < 2:
-            round_copies(level + 1)
         rows = level_rows(level)
+        if level == 0:
+            round_copies(1)
         for k in (2, 1, 3):
             remote(gathered.at[0, rows], gathered.at[Y - k, rows], WEIGHTS + level, (z, at_y(k), t)).start()
+        if level == 1:
+            round_copies(2)
 
     p, r = iota((128, 128), 0), iota((128, 128), 1)
     hlq = nt(one_hot(rank_of(query_order, p) == r), both[:, 0:128]).astype(BF16)
@@ -269,6 +269,9 @@
             hello(greet.at[1], (at_z(k), y, t))
         for k in (4, -4):
             remote(old.at[b], old.at[b], OLD, (at_z(k), y, t)).start()
+        arrived(ROUND, round_wait_shape(0))
+        round_copies(1)
+
         arrived(PART, from_y.at[pl.ds(0, 15)])
         summed = [from_y[0], part[y, odd]]
         for j in range(1, 2 * Y):
@@ -288,21 +291,22 @@
             z_copy(k)
 
         pl.semaphore_wait(greet.at[1], 2)
-        for k in (8, 4, 12, 2, 14):
+        z_copy(8)
+        remote(old.at[b], old.at[b], OLD, (at_z(8), y, t)).start()
+        for k in (4, 12, 2, 14):
             z_copy(k)
 
 
-        go_on(0)
-
-        arrived(OLD, old.at[pl.ds(0, 2)])
-        before = lax.rem(b + 3, 4)
-        remote(old.at[before], old.at[before], OLDER, (at_z(4), y, t)).start()
+        for k in (2, 1, 3):
+            remote(
+                gathered.at[0, level_rows(0)], gathered.at[Y - k, level_rows(0)], WEIGHTS, (z, at_y(k), t)
+            ).start()
 
         go_on(1)
 
         permuted_bases()
 
-        arrived(OLDER, old.at[0])
+        arrived(OLD, old.at[pl.ds(0, 3)])
         lower = iota((2, 128), 1) < 64
         for n in range(2):
             for i in (0, 2):
@@ -333,14 +337,14 @@
         there = 16 * xi + c
         def send_squares(dxs):
             for dx in dxs:
-                for k in (2, 1, -1, 0):
+                for k in (-2, 1, -1, 0):
                     for j in (2, 1, 3, 0):
                         for n in range(2):
                             if (dx, k, j, n) != (0, 0, 0, 1):
                                 remote(square, squares_o.at[there], SQUARES, (at_z(k), at_y(j), at_x(dx, n))).start()
 
         send_squares((2, 1, 3))
-        for k in (2, 1, -1, 0):
+        for k in (-2, 1, -1, 0):
             for j in (2, 1, 3, 0):
                 remote(send_ag.at[0, pl.ds(0, 3)], from_ag.at[c], DIRECTION_0, (at_z(k), at_y(j), t0)).start()
                 if (k, j) != (0, 0):
@@ -370,8 +374,7 @@
         left(DIRECTION, from_ag.at[pl.ds(0, 15)])
         left(DIRECTION_0, from_ag)
         left(MOMENTS, mom_o)
-        left(OLD, old.at[pl.ds(0, 2)])
-        left(OLDER, old.at[0])
+        left(OLD, old.at[pl.ds(0, 3)])
         weights_left()
         left(SQUARES, room)
 
@@ -382,9 +385,10 @@
 ):
     z, y = lax.axis_index("fs"), lax.axis_index("rep")
     b = lax.div(z, 4)
-    total = squares[0]
-    for k in range(1, 16 * X):
-        total = total + squares[k]
+    sums = [squares[k] for k in range(16 * X)]
+    while len(sums) > 1:
+        sums = [sums[k] + sums[k + 1] for k in range(0, len(sums), 2)]
+    total = sums[0]
     query_lanes = iota((1, 128), 1) < 64
     sum_q = jnp.sum(jnp.where(query_lanes, total, 0.0), axis=1, keepdims=True)
     sum_v = jnp.sum(jnp.where(query_lanes, 0.0, total), axis=1, keepdims=True)

time: 35.2 us -> 35 us (level)
  no operation moved by 1% of the time
where the time goes in v4:
time: 35 us; the launch traced here: 34.9 us
  Pallas kernels  34.2 us (98%)
  between operations  0.65 us (2%)
    pallas_call x1, Pallas kernels, body(): pl.pallas_call(exchange, out_shape=(shape((D, VL), F32), shape((D, QL), F...  33.1 us
    pallas_call x1, Pallas kernels, body(): pl.pallas_call(finish, out_shape=(shape((ROWS, QL), F32), shape((ROWS, VL...  1.11 us

profile of v4, /device:TPU:1, one launch (start us, length us, event | category | flops | bytes accessed | tf_op | source)
XLA Modules:
  0.0 34.9 jit_solution(16168784690904012498)
XLA Ops:
  0.6 33.1 %exchange.1 = (f32[1024,128]{1,0:T(8,128)S(1)}, f32[1024,64]{1,0:T(8,128)S(1)}, f32[1024,128]{1,0:T(8,128)S(1)}, f32[1024,128]{1,0:T(8,128)S(1)}, f32[2,3,4,128]...) custom-call(bf16[128,1024]{1,0:T(8,128)(2,1)} %x_h.1, bf16[64,128]{1,0:T(8,128)(2,1)} %bitcast.2, bf16[128,128]{1,0:T(8,128)(2,1)} %cv_h.1, ...), custom_call_target="tpu_custom_call" | custom-call | tf_op jit(solution)/shard_map/exchange/pallas_call | solution.py:427
  33.8 1.1 %finish.1 = (f32[16,64]{1,0:T(8,128)}, f32[16,128]{1,0:T(8,128)}, f32[16,64]{1,0:T(8,128)}, f32[16,128]{1,0:T(8,128)}, f32[2,64]{1,0:T(2,128)}, /*index=5*/f32[2...) custom-call(f32[1024,128]{1,0:T(8,128)S(1)} %get-tuple-element.26.uv, ...), custom_call_target="tpu_custom_call" | custom-call | tf_op jit(solution)/shard_map/finish/pallas_call | solution.py:454

commit v5 on v4

--- a/solution.py
+++ b/solution.py
@@ -104,7 +104,7 @@
         pl.semaphore_signal(semaphore, inc=1, device_id=device, device_id_type=MESH)
 
     barrier = pltpu.get_barrier_semaphore()
-    for k in range(Y):
+    for k in (2, 1, 3, 0):
         @pl.when(core == 1)
         def _():
             hello(barrier, (z, at_y(k), t0))
@@ -196,6 +196,8 @@
         pl.semaphore_wait(barrier, 17)
         remote(own_old, old.at[b, 0], OWN_OLD, (z, y, t1)).start()
 
+    round_copies(0)
+
     def part_copy(n, k):
         slot = 2 * (Y * n + (Y - k) % Y) + core
         there, parity = (mate, 1 - odd) if n else (z, odd)
@@ -209,8 +211,6 @@
     @pl.when(core == 0)
     def _():
         part_copy(0, 0)
-
-    round_copies(0)
 
     def permuted_bases():
         r, p = iota((128, 256), 0), iota((128, 256), 1) & 127
@@ -335,21 +335,33 @@
         row = jnp.where(iota((1, 128), 1) < 64, square_q, square_v)
         square[...] = row
         there = 16 * xi + c
-        def send_squares(dxs):
+        def send_squares(k, dxs):
             for dx in dxs:
-                for k in (-2, 1, -1, 0):
-                    for j in (2, 1, 3, 0):
-                        for n in range(2):
-                            if (dx, k, j, n) != (0, 0, 0, 1):
-                                remote(square, squares_o.at[there], SQUARES, (at_z(k), at_y(j), at_x(dx, n))).start()
-
-        send_squares((2, 1, 3))
-        for k in (-2, 1, -1, 0):
-            for j in (2, 1, 3, 0):
-                remote(send_ag.at[0, pl.ds(0, 3)], from_ag.at[c], DIRECTION_0, (at_z(k), at_y(j), t0)).start()
-                if (k, j) != (0, 0):
-                    remote(send_ag.at[0, pl.ds(3, 3)], from_ag.at[c], DIRECTION, (at_z(k), at_y(j), t)).start()
-        send_squares((0,))
+                for j in (0, 2, 1, 3):
+                    for n in range(2):
+                        one = remote(square, squares_o.at[there], SQUARES, (at_z(k), j, at_x(dx, n)))
+                        if (dx, k, n) == (0, 0, 1):
+                            pl.when(y != j)(one.start)
+                        else:
+                            one.start()
+
+        def send_out(k):
+            send_squares(k, (2,))
+            for j in (0, 2, 1, 3):
+                one = remote(send_ag.at[0, pl.ds(3, 3)], from_ag.at[c], DIRECTION, (at_z(k), j, t))
+                if k:
+                    one.start()
+                else:
+                    pl.when(y != j)(one.start)
+                remote(send_ag.at[0, pl.ds(0, 3)], from_ag.at[c], DIRECTION_0, (at_z(k), j, t0)).start()
+            send_squares(k, (1, 3, 0))
+
+        for first in (True, False):
+            for k in (-2, 1, -1, 0):
+                @pl.when((at_z(k) == 0) if first else (at_z(k) != 0))
+                def _():
+                    send_out(k)
+
         squares_o[there] = row
         from_ag[c] = direction[3:6]
         send_ag[1] = first_new

time: 35 us -> 34.1 us (0.974)
  Pallas kernels: 34.2 us -> 33.4 us
    pallas_call x1, Pallas kernels: 33.1 us -> 32.2 us  [body(): pl.pallas_call(exchange, out_shape=(shape((D, VL), F32), shape((D, QL), F...]
where the time goes in v5:
time: 34.1 us; the launch traced here: 34 us
  Pallas kernels  33.4 us (98%)
  between operations  0.65 us (2%)
    pallas_call x1, Pallas kernels, body(): pl.pallas_call(exchange, out_shape=(shape((D, VL), F32), shape((D, QL), F...  32.2 us
    pallas_call x1, Pallas kernels, body(): pl.pallas_call(finish, out_shape=(shape((ROWS, QL), F32), shape((ROWS, VL...  1.11 us

profile of v5, /device:TPU:1, one launch (start us, length us, event | category | flops | bytes accessed | tf_op | source)
XLA Modules:
  0.0 34.0 jit_solution(13665228285130626762)
XLA Ops:
  0.6 32.2 %exchange.1 = (f32[1024,128]{1,0:T(8,128)S(1)}, f32[1024,64]{1,0:T(8,128)S(1)}, f32[1024,128]{1,0:T(8,128)S(1)}, f32[1024,128]{1,0:T(8,128)S(1)}, f32[2,3,4,128]...) custom-call(bf16[128,1024]{1,0:T(8,128)(2,1)} %x_h.1, bf16[64,128]{1,0:T(8,128)(2,1)} %bitcast.2, bf16[128,128]{1,0:T(8,128)(2,1)} %cv_h.1, ...), custom_call_target="tpu_custom_call" | custom-call | tf_op jit(solution)/shard_map/exchange/pallas_call | solution.py:439
  32.9 1.1 %finish.1 = (f32[16,64]{1,0:T(8,128)}, f32[16,128]{1,0:T(8,128)}, f32[16,64]{1,0:T(8,128)}, f32[16,128]{1,0:T(8,128)}, f32[2,64]{1,0:T(2,128)}, /*index=5*/f32[2...) custom-call(f32[1024,128]{1,0:T(8,128)S(1)} %get-tuple-element.26.uv, ...), custom_call_target="tpu_custom_call" | custom-call | tf_op jit(solution)/shard_map/finish/pallas_call | solution.py:466
